TPU v7x, 32 devices: a whole 2x2x4 slice. The times are simulated.
32 devices in a mesh: sp: 8 (over z, x), tp: 4 (over y, core).
Axes of the slice: x: 2, y: 2, z: 4, core: 2. Of those that a mesh axis runs over, the one named last changes fastest.
Arguments:
- tokens: bfloat16 [4096, 2048], P(('sp', 'tp')), may hold values from -8 to 8
- in_gain: float32 [2048], replicated, may hold values from 0.1 to 1.9
- w_conv_val: bfloat16 [2048, 1024], P('sp', 'tp'), may hold values from -0.125 to 0.125
- w_conv_gate: bfloat16 [2048, 1024], P('sp', 'tp'), may hold values from -0.125 to 0.125
- w_query: bfloat16 [2048, 1024], P('sp', 'tp'), may hold values from -1 to 1
- w_key: bfloat16 [2048, 256], P('sp', 'tp'), may hold values from -1 to 1
- value_weight: bfloat16 [2048, 256], P('sp', 'tp'), may hold values from -0.125 to 0.125
- conv_taps: float32 [31, 1024], P(None, 'tp'), may hold values from -1 to 1
- conv_bias: float32 [1024], P('tp'), may hold values from -3 to 3
- norm_gain: float32 [1024], P('tp'), may hold values from 0.1 to 1.9
- norm_bias: float32 [1024], P('tp'), may hold values from -3 to 3
- head_sink_logit: float32 [16], P('tp'), may hold values from 4 to 7
- w_out_conv: bfloat16 [1024, 2048], P('tp', 'sp'), may hold values from -0.125 to 0.125
- w_out_attn: bfloat16 [1024, 2048], P('tp', 'sp'), may hold values from -0.125 to 0.125
Outputs:
- mixed: bfloat16 [4096, 2048], P(('sp', 'tp'))
- log_total: float32 [4096, 16], P('sp', 'tp')
All inputs are finite; a program needn't handle non-finite values.
Results may differ from a plain program's by a relative error of at most 0.012.
Values may be sent and summed in bfloat16 or wider, within the bound.
A program may use at most 64 MiB of HBM per device.

v0:
```python
import functools

import jax
import jax.numpy as jnp
from jax import lax
from jax.experimental import pallas as pl
from jax.experimental.pallas import tpu as pltpu
from jax.sharding import PartitionSpec as P

WINDOW_REACH = 128


def with_halo(cells, sides, width):
    for axis, dim in sides:
        count = lax.axis_size(axis)
        ends = count - 1
        head = lax.slice_in_dim(cells, 0, width, axis=dim)
        tail = lax.slice_in_dim(cells, cells.shape[dim] - width, cells.shape[dim], axis=dim)
        cells = jnp.concatenate(
            [
                lax.ppermute(tail, axis, [(i, (i + 1) % count) for i in range(ends)]),
                cells,
                lax.ppermute(head, axis, [((i + 1) % count, i) for i in range(ends)]),
            ],
            axis=dim,
        )
    return cells


def on_device(
    tokens,
    in_gain,
    w_conv_val,
    w_conv_gate,
    w_query,
    w_key,
    value_weight,
    conv_taps,
    conv_bias,
    norm_gain,
    norm_bias,
    head_sink_logit,
    w_out_conv,
    w_out_attn,
):
    flt = tokens.astype(jnp.float32)
    normed = (
        flt * lax.rsqrt(jnp.mean(flt * flt, axis=-1, keepdims=True) + 1e-06) * in_gain
    ).astype(jnp.bfloat16)
    val_full, gate_full, query_full, key_full, value_full = (
        lax.all_gather(w_conv_val, "sp", axis=0, tiled=True),
        lax.all_gather(w_conv_gate, "sp", axis=0, tiled=True),
        lax.all_gather(w_query, "sp", axis=0, tiled=True),
        lax.all_gather(w_key, "sp", axis=0, tiled=True),
        lax.all_gather(value_weight, "sp", axis=0, tiled=True),
    )
    joined = jnp.concatenate([val_full, gate_full, query_full, key_full, value_full], axis=1)
    projected = jnp.dot(
        lax.all_gather(normed, "tp", axis=0, tiled=True), joined, preferred_element_type=jnp.float32
    )
    chans = val_full.shape[1]
    qwidth = query_full.shape[1]
    kwidth = key_full.shape[1]
    length = projected.shape[0]
    glu = (projected[:, :chans] * jax.nn.sigmoid(projected[:, chans : 2 * chans])).astype(
        jnp.bfloat16
    )
    base = 2 * chans
    query_matrix = projected[:, base : base + qwidth].astype(jnp.bfloat16)
    key = projected[:, base + qwidth : base + qwidth + kwidth].astype(jnp.bfloat16)
    value_matrix = projected[:, base + qwidth + kwidth :].astype(jnp.bfloat16)
    taps = conv_taps.shape[0]
    half = taps // 2
    padded = with_halo(glu, (("sp", 0),), half)
    filtered = jnp.zeros(glu.shape, jnp.float32) + conv_bias
    for offset in range(taps):
        filtered = (
            filtered + padded[offset : offset + length].astype(jnp.float32) * conv_taps[offset]
        )
    sums, squares = lax.psum(
        (jnp.sum(filtered, axis=-1), jnp.sum(filtered * filtered, axis=-1)), "tp"
    )
    count = chans * lax.axis_size("tp")
    center = (sums / count)[:, None]
    spread = (squares / count)[:, None] - center * center
    conv_out = jax.nn.silu(
        (filtered - center) * lax.rsqrt(spread + 1e-05) * norm_gain + norm_bias
    ).astype(jnp.bfloat16)
    heads_here = head_sink_logit.shape[0]
    head_size = qwidth // heads_here
    kv_here = kwidth // head_size
    query_groups = heads_here // kv_here
    stacked = jnp.stack([key, value_matrix], axis=0)
    banded = with_halo(stacked, (("sp", 1),), WINDOW_REACH)
    span = length + 2 * WINDOW_REACH
    key_band = banded[0].reshape(span, kv_here, head_size)
    value_band = banded[1].reshape(span, kv_here, head_size)
    query4_grouped = query_matrix.reshape(length, kv_here, query_groups, head_size)
    scores = jnp.einsum(
        "qkgd,jkd->kgqj", query4_grouped, key_band, preferred_element_type=jnp.float32
    ) * head_size ** (-0.5)
    offset_pos = lax.axis_index("sp") * length
    seq_len = length * lax.axis_size("sp")
    qpos = offset_pos + jnp.arange(length, dtype=jnp.int32)
    kpos = offset_pos - WINDOW_REACH + jnp.arange(span, dtype=jnp.int32)
    valid = (
        (jnp.abs(qpos[:, None] - kpos[None, :]) <= WINDOW_REACH)
        & (kpos[None, :] >= 0)
        & (kpos[None, :] < seq_len)
    )
    sink_column = head_sink_logit.reshape(kv_here, query_groups, 1)
    masked = jnp.where(valid, scores, -1e30)
    top = jnp.maximum(jnp.max(masked, axis=-1), sink_column)
    expd = jnp.where(valid, jnp.exp(masked - top[..., None]), 0.0)
    total = jnp.sum(expd, axis=-1) + jnp.exp(sink_column - top)
    probs = (expd / total[..., None]).astype(jnp.bfloat16)
    attended = jnp.einsum(
        "kgqj,jkd->qkgd", probs, value_band, preferred_element_type=jnp.float32
    ).astype(jnp.bfloat16)
    attended = attended.reshape(length, qwidth)
    log_total = (top + jnp.log(total)).reshape(heads_here, length).T
    out_conv_cols, out_attn_cols = (
        lax.all_gather(w_out_conv, "sp", axis=1, tiled=True),
        lax.all_gather(w_out_attn, "sp", axis=1, tiled=True),
    )
    out_rows = jnp.concatenate([out_conv_cols, out_attn_cols], axis=0)
    features = jnp.concatenate([conv_out, attended], axis=1)
    mixed = lax.psum_scatter(
        jnp.dot(features, out_rows, preferred_element_type=jnp.float32).astype(jnp.bfloat16),
        "tp",
        scatter_dimension=0,
        tiled=True,
    )
    return (mixed, log_total)


BF = jnp.bfloat16
F32 = jnp.float32


def fused_kernel(
    n, x_hbm, gain, wval, wgate, wquery, wkey, wvalue, taps, cbias, ngain, nbias, sink, woc, woa,
    mixed, logt,
    tok, nrm, wq, wc, wo, accq, accc, qb, band, glu, filt, stat, feat, part,
    p1s, p1r, p2s, p2r, own,
    lsem, tsem, trec, rsem, rrec, hsem, hrec, ssem, srec, asem, arec, bsem, brec,
):
    sp = lax.axis_index("sp")
    t = lax.axis_index("tp")
    half = n // 2
    tl, width = x_hbm.shape
    length = 4 * tl
    kb = wval.shape[0]
    chans = wval.shape[1]
    qwidth = wquery.shape[1]
    hd = wkey.shape[0]
    kvw = 2 * hd
    heads = sink.shape[1]
    ob = woc.shape[1]
    reach = WINDOW_REACH
    y, c = t // 2, t % 2
    core_peer = y * 2 + 1 - c
    y_peer = (1 - y) * 2 + c
    far_peer = (1 - y) * 2 + 1 - c
    xbit, zpos = sp % 2, sp // 2
    pos = (1 - xbit) * zpos + xbit * (n - 1 - zpos)

    def at_pos(q):
        q = (q + 2 * n) % n
        hi = q // half
        return (1 - hi) * (2 * q) + hi * (2 * (n - 1 - q) + 1)

    right, left = at_pos(pos + 1), at_pos(pos - 1)
    nxt, prv = (sp + 1) % n, (sp + n - 1) % n

    def rows(o, size):
        return pl.ds(pl.multiple_of(o * size, size), size)

    local = [
        pltpu.make_async_copy(x_hbm, tok.at[rows(t, tl)], lsem.at[0]),
        pltpu.make_async_copy(wquery, wq.at[sp, pl.ds(0, kb)], lsem.at[1]),
        pltpu.make_async_copy(wkey, wq.at[sp, pl.ds(kb, hd)], lsem.at[2]),
        pltpu.make_async_copy(wvalue, wq.at[sp, pl.ds(kb + hd, hd)], lsem.at[7]),
        pltpu.make_async_copy(wval, wc.at[rows(sp, kb), pl.ds(0, chans)], lsem.at[3]),
        pltpu.make_async_copy(wgate, wc.at[rows(sp, kb), pl.ds(chans, chans)], lsem.at[4]),
        pltpu.make_async_copy(woc, wo.at[sp, pl.ds(0, chans)], lsem.at[5]),
        pltpu.make_async_copy(woa, wo.at[sp, pl.ds(chans, qwidth)], lsem.at[6]),
    ]
    for cp in local:
        cp.start()
    barrier = pltpu.get_barrier_semaphore()
    for dev in (right, left, nxt, prv):
        pl.semaphore_signal(
            barrier, inc=1, device_id={"sp": dev}, device_id_type=pl.DeviceIdType.MESH
        )
    for dev in (core_peer, y_peer, far_peer):
        pl.semaphore_signal(
            barrier, inc=1, device_id={"tp": dev}, device_id_type=pl.DeviceIdType.MESH
        )
    pl.semaphore_wait(barrier, 7)

    sent = []

    def remote(src, dst, ss, rs, dev):
        cp = pltpu.make_async_remote_copy(
            src_ref=src, dst_ref=dst, send_sem=ss, recv_sem=rs, device_id=dev,
            device_id_type=pl.DeviceIdType.MESH,
        )
        cp.start()
        sent.append(cp)
        return cp

    ring = {}

    def block_ref(k, o, h):
        if k == 0:
            depth = wq.shape[1] // 2
            return wq.at[o, pl.ds(h * depth, depth)]
        if k == 1:
            return wc.at[pl.ds(pl.multiple_of(o * kb + h * (kb // 2), kb // 2), kb // 2)]
        depth = wo.shape[1] // 2
        return wo.at[o, pl.ds(h * depth, depth)]

    def ring_event(k, s, halves=(0, 1)):
        for h in halves:
            for d in (0, 1):
                if s > 1:
                    ring[k, d, s - 1, h].wait_recv()
                if s < half or h == d:
                    o = at_pos(pos - (s - 1) if d == 0 else pos + (s - 1))
                    ref = block_ref(k, o, h)
                    ring[k, d, s, h] = remote(
                        ref, ref, rsem.at[k, d, s - 1, h], rrec.at[k, d, s - 1, h],
                        {"sp": right if d == 0 else left},
                    )

    def ring_last(k):
        for d in (0, 1):
            ring[k, d, half, d].wait_recv()

    def owners(s):
        if s == 0:
            return [sp]
        if s == half:
            return [at_pos(pos + half)]
        return [at_pos(pos - s), at_pos(pos + s)]

    local[4].wait()
    local[5].wait()
    ring_event(1, 1)
    local[0].wait()
    hl = tl // 2
    tokcp = {}

    def tok_send(slot, h, e, dev):
        ref = tok.at[pl.ds(pl.multiple_of(slot * tl + h * hl, hl), hl)]
        tokcp[e, h] = remote(ref, ref, tsem.at[e, h], trec.at[e, h], {"tp": dev})

    for h in (0, 1):
        tok_send(t, h, 0, y_peer)
    for h in (0, 1):
        tok_send(t, h, 1, core_peer)
    for i in (1, 2, 3, 6, 7):
        local[i].wait()

    def norm_rows(slot):
        step = 32

        def body(i, carry):
            r = pl.ds(pl.multiple_of(slot * tl + i * step, step), step)
            flt = tok[r, :].astype(F32)
            scale = lax.rsqrt(jnp.mean(flt * flt, axis=-1, keepdims=True) + 1e-06)
            nrm[r, :] = (flt * scale * gain[...]).astype(BF)
            return carry

        lax.fori_loop(0, tl // step, body, 0)

    norm_rows(t)
    for h in (0, 1):
        tokcp[1, h].wait_recv()
    ring_event(1, 2, (0,))
    norm_rows(core_peer)
    ring_event(1, 2, (1,))
    tokcp[0, 0].wait_recv()
    tok_send(y_peer, 0, 2, core_peer)
    ring_event(1, 3, (0,))
    ring_event(1, 3, (1,))
    tokcp[0, 1].wait_recv()
    tok_send(y_peer, 1, 2, core_peer)
    ring_event(0, 1, (0,))
    norm_rows(y_peer)
    for h in (0, 1):
        tokcp[2, h].wait_recv()
    norm_rows(far_peer)

    def columns(o):
        return nrm[:, pl.ds(pl.multiple_of(o * kb, kb), kb)]

    def project_conv(s):
        for o in owners(s):
            res = jnp.dot(columns(o), wc[rows(o, kb), :], preferred_element_type=F32)
            accc[...] = res if s == 0 else accc[...] + res

    def project_heads(s):
        for o in owners(s):
            lhs = columns(o)
            res = jnp.dot(lhs, wq[o, 0:kb, :], preferred_element_type=F32)
            two = lax.dot_general(
                lhs, wq[o, kb : kb + kvw, :], (((1,), (1,)), ((), ())),
                preferred_element_type=F32,
            )
            if s == 0:
                accq[:, 0:qwidth] = res
                accq[:, qwidth : qwidth + kvw] = two
            else:
                accq[:, 0:qwidth] = accq[:, 0:qwidth] + res
                accq[:, qwidth : qwidth + kvw] = accq[:, qwidth : qwidth + kvw] + two

    project_conv(0)
    ring_event(1, 4)
    ring_event(0, 1, (1,))
    project_conv(1)
    project_conv(2)
    project_conv(3)
    ring_event(0, 2, (0,))
    ring_last(1)
    project_conv(4)
    pad = 16
    glu[pl.ds(pad, length), :] = (
        (accc[:, 0:chans] * jax.nn.sigmoid(accc[:, chans : 2 * chans])).astype(BF).astype(F32)
    )
    g_up = remote(
        glu.at[pl.ds(length, pad)], glu.at[pl.ds(0, pad)], hsem.at[2], hrec.at[2], {"sp": nxt}
    )
    g_down = remote(
        glu.at[pl.ds(pad, pad)], glu.at[pl.ds(length + pad, pad)], hsem.at[3], hrec.at[3],
        {"sp": prv},
    )
    ring_event(0, 2, (1,))
    ntaps = taps.shape[0]
    off = pad - ntaps // 2
    cstep = 64

    def conv_rows(r0):
        acc = jnp.zeros((cstep, chans), F32) + cbias[...]
        for j in range(ntaps):
            acc = acc + glu[pl.ds(r0 + off + j, cstep), :] * taps[pl.ds(j, 1), :]
        filt[pl.ds(r0, cstep), :] = acc

    nconv = length // cstep
    for i in range(1, nconv - 1):
        conv_rows(i * cstep)
    ring_event(0, 3)
    g_up.wait_recv()
    g_down.wait_recv()

    @pl.when(sp == 0)
    def _():
        glu[pl.ds(0, pad), :] = jnp.zeros((pad, chans), F32)

    @pl.when(sp == n - 1)
    def _():
        glu[pl.ds(length + pad, pad), :] = jnp.zeros((pad, chans), F32)

    conv_rows(0)
    conv_rows((nconv - 1) * cstep)
    lane = lax.broadcasted_iota(jnp.int32, (128, 128), 1)
    for b in range(length // 128):
        f = filt[pl.ds(b * 128, 128), :]
        s1 = jnp.sum(f, axis=-1, keepdims=True)
        s2 = jnp.sum(f * f, axis=-1, keepdims=True)
        tile = jnp.where(lane == 0, s1, jnp.where(lane == 1, s2, 0.0))
        stat[pl.ds(t, 1), :, pl.ds(b * 128, 128)] = jnp.transpose(tile)[None, 0:8, :]
    scp = []
    for e, dev in enumerate((y_peer, far_peer, core_peer)):
        scp.append(remote(stat.at[t], stat.at[t], ssem.at[e], srec.at[e], {"tp": dev}))
    ring_event(2, 1, (0,))
    ring_event(0, 4)
    ring_event(2, 1, (1,))
    project_heads(0)
    project_heads(1)
    project_heads(2)
    for cp in scp:
        cp.wait_recv()
    count = chans * 4
    for b in range(length // 128):
        cols = pl.ds(b * 128, 128)
        tot = (stat[0, :, cols] + stat[1, :, cols] + stat[2, :, cols] + stat[3, :, cols]) / count
        tt = jnp.transpose(jnp.concatenate([tot] * 16, axis=0))
        center = tt[:, 0:1]
        spread = tt[:, 1:2] - center * center
        u = (filt[pl.ds(b * 128, 128), :] - center) * lax.rsqrt(spread + 1e-05)
        u = u * ngain[...] + nbias[...]
        feat[pl.ds(b * 128, 128), 0:chans] = (u * jax.nn.sigmoid(u)).astype(BF)

    project_heads(3)
    ring_last(0)
    project_heads(4)
    qb[...] = accq[:, 0:qwidth].astype(BF)
    band[pl.ds(reach, length), :] = accq[:, qwidth : qwidth + kvw].astype(BF)
    kv_up = remote(
        band.at[pl.ds(length, reach)], band.at[pl.ds(0, reach)], hsem.at[0], hrec.at[0],
        {"sp": nxt},
    )
    kv_down = remote(
        band.at[pl.ds(reach, reach)], band.at[pl.ds(length + reach, reach)], hsem.at[1],
        hrec.at[1], {"sp": prv},
    )
    seq_len = length * n

    def attend(b):
        blk = reach
        span = blk + 2 * reach
        kk = band[pl.ds(b * blk, span), 0:hd]
        vv = band[pl.ds(b * blk, span), hd:kvw]
        ri = lax.broadcasted_iota(jnp.int32, (blk, span), 0)
        ci = lax.broadcasted_iota(jnp.int32, (blk, span), 1)
        kp = sp * length + b * blk - reach + ci
        valid = (ci >= ri) & (ci <= ri + 2 * reach) & (kp >= 0) & (kp < seq_len)
        logs = []
        for h in range(heads):
            q = qb[pl.ds(b * blk, blk), h * hd : (h + 1) * hd]
            s = lax.dot_general(
                q, kk, (((1,), (1,)), ((), ())), preferred_element_type=F32
            ) * hd ** (-0.5)
            s = jnp.where(valid, s, -1e30)
            sk = sink[0:1, h : h + 1]
            top = jnp.maximum(jnp.max(s, axis=-1, keepdims=True), sk)
            e = jnp.where(valid, jnp.exp(s - top), 0.0)
            total = jnp.sum(e, axis=-1, keepdims=True) + jnp.exp(sk - top)
            p = (e * (1.0 / total)).astype(BF)
            a = jnp.dot(p, vv, preferred_element_type=F32).astype(BF)
            feat[pl.ds(b * blk, blk), chans + h * hd : chans + (h + 1) * hd] = a
            logs.append(top + jnp.log(total))
        wide = jnp.zeros((blk, 128), F32)
        for h in range(heads):
            wide = jnp.where(lane == h, logs[h], wide)
        logt[:, pl.ds(b * blk, blk)] = jnp.transpose(wide)[0:heads, :]

    nblk = length // reach
    attend(1)
    ring_event(2, 2)
    for b in range(2, nblk - 1):
        attend(b)
    kv_up.wait_recv()
    kv_down.wait_recv()
    attend(0)
    attend(nblk - 1)

    acp, bcp = {}, {}
    order = []

    def emit(o):
        i = len(order)
        order.append(o)
        part[...] = jnp.dot(feat[...], wo[o], preferred_element_type=F32)
        p1s[i, pl.ds(0, tl), :] = part[rows(core_peer, tl), :].astype(BF)
        p1s[i, pl.ds(tl, tl), :] = part[rows(far_peer, tl), :].astype(BF)
        acp[i] = remote(p1s.at[i], p1r.at[i], asem.at[i], arec.at[i], {"tp": core_peer})
        own[i, pl.ds(0, tl), :] = part[rows(t, tl), :]
        own[i, pl.ds(tl, tl), :] = part[rows(y_peer, tl), :]

    def cross(i):
        acp[i].wait_recv()
        p2s[i] = (own[i, pl.ds(tl, tl), :] + p1r[i, pl.ds(tl, tl), :].astype(F32)).astype(BF)
        bcp[i] = remote(p2s.at[i], p2r.at[i], bsem.at[i], brec.at[i], {"tp": y_peer})

    def finish(i):
        bcp[i].wait_recv()
        mixed[:, rows(order[i], ob)] = (
            own[i, pl.ds(0, tl), :] + p1r[i, pl.ds(0, tl), :].astype(F32)
            + p2r[i].astype(F32)
        ).astype(BF)

    def out_step(s):
        for o in owners(s):
            emit(o)
            if len(order) >= 2:
                cross(len(order) - 2)

    out_step(0)
    ring_event(2, 3)
    out_step(1)
    out_step(2)
    ring_event(2, 4)
    out_step(3)
    ring_last(2)
    out_step(half)
    cross(n - 1)
    for i in range(n):
        finish(i)
    for cp in sent:
        cp.wait_send()


def layer(
    n, parts, tokens, in_gain, w_conv_val, w_conv_gate, w_query, w_key, value_weight, conv_taps,
    conv_bias, norm_gain, norm_bias, head_sink_logit, w_out_conv, w_out_attn,
):
    tl, width = tokens.shape
    kb, chans = w_conv_val.shape
    qwidth = w_query.shape[1]
    kvw = 2 * w_key.shape[1]
    heads = head_sink_logit.shape[0]
    ob = w_out_conv.shape[1]
    fits = (
        parts == 4 and n == 8 and tl % 128 == 0 and kb % 128 == 0 and ob % 128 == 0
        and chans % 128 == 0 and kvw == 128 and kb == qwidth and qwidth == heads * kvw // 2
        and conv_taps.shape[0] <= 33
    )
    if not fits:
        return on_device(
            tokens, in_gain, w_conv_val, w_conv_gate, w_query, w_key, value_weight, conv_taps,
            conv_bias, norm_gain, norm_bias, head_sink_logit, w_out_conv, w_out_attn,
        )
    length = 4 * tl
    half = n // 2
    vm = pl.BlockSpec(memory_space=pltpu.VMEM)
    hb = pl.BlockSpec(memory_space=pl.ANY)
    dma = pltpu.SemaphoreType.DMA
    mixed, log_rows = pl.pallas_call(
        functools.partial(fused_kernel, n),
        out_shape=(
            jax.ShapeDtypeStruct((tl, width), BF),
            jax.ShapeDtypeStruct((heads, length), F32),
        ),
        in_specs=[hb, vm, hb, hb, hb, hb, hb, vm, vm, vm, vm, vm, hb, hb],
        out_specs=(vm, vm),
        scratch_shapes=[
            pltpu.VMEM((length, width), BF),
            pltpu.VMEM((length, width), BF),
            pltpu.VMEM((n, kb + kvw, qwidth), BF),
            pltpu.VMEM((n * kb, 2 * chans), BF),
            pltpu.VMEM((n, chans + qwidth, ob), BF),
            pltpu.VMEM((length, qwidth + kvw), F32),
            pltpu.VMEM((length, 2 * chans), F32),
            pltpu.VMEM((length, qwidth), BF),
            pltpu.VMEM((length + 2 * WINDOW_REACH, kvw), BF),
            pltpu.VMEM((length + 32, chans), F32),
            pltpu.VMEM((length, chans), F32),
            pltpu.VMEM((4, 8, length), F32),
            pltpu.VMEM((length, chans + qwidth), BF),
            pltpu.VMEM((length, ob), F32),
            pltpu.VMEM((n, 2 * tl, ob), BF),
            pltpu.VMEM((n, 2 * tl, ob), BF),
            pltpu.VMEM((n, tl, ob), BF),
            pltpu.VMEM((n, tl, ob), BF),
            pltpu.VMEM((n, 2 * tl, ob), F32),
            dma((8,)),
            dma((3, 2)),
            dma((3, 2)),
            dma((3, 2, half, 2)),
            dma((3, 2, half, 2)),
            dma((4,)),
            dma((4,)),
            dma((3,)),
            dma((3,)),
            dma((n,)),
            dma((n,)),
            dma((n,)),
            dma((n,)),
        ],
        compiler_params=pltpu.CompilerParams(
            collective_id=0, has_side_effects=True, vmem_limit_bytes=56 * 1024 * 1024
        ),
    )(
        tokens, in_gain.reshape(1, width), w_conv_val, w_conv_gate, w_query, w_key.T, value_weight.T,
        conv_taps, conv_bias.reshape(1, chans), norm_gain.reshape(1, chans), norm_bias.reshape(1, chans),
        head_sink_logit.reshape(1, heads), w_out_conv, w_out_attn,
    )
    return mixed, log_rows.T


def solution(mesh):
    return jax.shard_map(
        functools.partial(layer, mesh.shape["sp"], mesh.shape["tp"]),
        mesh=mesh,
        in_specs=(
            P(("sp", "tp"), None),
            P(),
            P("sp", "tp"),
            P("sp", "tp"),
            P("sp", "tp"),
            P("sp", "tp"),
            P("sp", "tp"),
            P(None, "tp"),
            P("tp"),
            P("tp"),
            P("tp"),
            P("tp"),
            P("tp", "sp"),
            P("tp", "sp"),
        ),
        out_specs=(P(("sp", "tp"), None), P("sp", "tp")),
        check_vma=False,
    )
```

profile of v0, /device:TPU:0, one launch (start us, length us, event | category | flops | bytes accessed | tf_op | source)
XLA Modules:
  0.0 77.4 jit_solution(3443548451948539687)
XLA Ops:
  0.6 74.3 %shard_map.149 = (bf16[128,2048]{1,0:T(8,128)(2,1)}, f32[4,512]{1,0:T(4,128)}) custom-call(bf16[128,2048]{1,0:T(8,128)(2,1)} %x_hbm.1, f32[1,2048]{1,0:T(1,128)} %bitcast.10, bf16[256,256]{1,0:T(8,128)(2,1)} %wval.1, bf16[256,256]{1,0:T(8,128)(2,1)} %wgate.1, bf16[256,256]{1,0:T(8,128)(2,1)} %wquery.1, bf16[64,256]{1,0:T(8,128)(2,1)} %bitcast.8, ...), custom_call_target="tpu_custom_call" | custom-call | tf_op jit(solution)/shard_map/pallas_call | solution.py:521
  74.9 0.0 copy-start
  74.9 1.9 %copy.18 = bf16[128,2048]{1,0:T(8,128)(2,1)} copy(bf16[128,2048]{1,0:T(8,128)(2,1)} %get-tuple-element.8) | data formatting | bytes 1048576
  76.8 0.0 copy-done
  76.8 0.6 copy.19
Async XLA Ops:
  74.9 1.9 %copy-start = (f32[4,512]{1,0:T(4,128)S(1)}, f32[4,512]{1,0:T(4,128)}, u32[]{:S(2)}) copy-start(f32[4,512]{1,0:T(4,128)} %get-tuple-element.5) | copy-start | bytes 24580
where the time goes:
time: 77.6 us; the launch traced here: 77.4 us
  Pallas kernels  74.3 us (96%)
  local copies, waits for them, and re-layouts  2.49 us (3%)
    pallas_call x1, Pallas kernels, layer(): pl.pallas_call(functools.partial(fused_kernel, n), out_shape=(jax.ShapeDt...  74.3 us
    unnamed x4, local copies, waits for them, and re-layouts  2.49 us

commit v1 on v0

v1 whole, which is shorter than its diff:
```python
import functools

import jax
import jax.numpy as jnp
from jax import lax
from jax.experimental import pallas as pl
from jax.experimental.pallas import tpu as pltpu
from jax.sharding import PartitionSpec as P

WINDOW_REACH = 128


def with_halo(cells, sides, width):
    for axis, dim in sides:
        count = lax.axis_size(axis)
        ends = count - 1
        head = lax.slice_in_dim(cells, 0, width, axis=dim)
        tail = lax.slice_in_dim(cells, cells.shape[dim] - width, cells.shape[dim], axis=dim)
        cells = jnp.concatenate(
            [
                lax.ppermute(tail, axis, [(i, (i + 1) % count) for i in range(ends)]),
                cells,
                lax.ppermute(head, axis, [((i + 1) % count, i) for i in range(ends)]),
            ],
            axis=dim,
        )
    return cells


def on_device(
    tokens,
    in_gain,
    w_conv_val,
    w_conv_gate,
    w_query,
    w_key,
    value_weight,
    conv_taps,
    conv_bias,
    norm_gain,
    norm_bias,
    head_sink_logit,
    w_out_conv,
    w_out_attn,
):
    flt = tokens.astype(jnp.float32)
    normed = (
        flt * lax.rsqrt(jnp.mean(flt * flt, axis=-1, keepdims=True) + 1e-06) * in_gain
    ).astype(jnp.bfloat16)
    val_full, gate_full, query_full, key_full, value_full = (
        lax.all_gather(w_conv_val, "sp", axis=0, tiled=True),
        lax.all_gather(w_conv_gate, "sp", axis=0, tiled=True),
        lax.all_gather(w_query, "sp", axis=0, tiled=True),
        lax.all_gather(w_key, "sp", axis=0, tiled=True),
        lax.all_gather(value_weight, "sp", axis=0, tiled=True),
    )
    joined = jnp.concatenate([val_full, gate_full, query_full, key_full, value_full], axis=1)
    projected = jnp.dot(
        lax.all_gather(normed, "tp", axis=0, tiled=True), joined, preferred_element_type=jnp.float32
    )
    chans = val_full.shape[1]
    qwidth = query_full.shape[1]
    kwidth = key_full.shape[1]
    length = projected.shape[0]
    glu = (projected[:, :chans] * jax.nn.sigmoid(projected[:, chans : 2 * chans])).astype(
        jnp.bfloat16
    )
    base = 2 * chans
    query_matrix = projected[:, base : base + qwidth].astype(jnp.bfloat16)
    key = projected[:, base + qwidth : base + qwidth + kwidth].astype(jnp.bfloat16)
    value_matrix = projected[:, base + qwidth + kwidth :].astype(jnp.bfloat16)
    taps = conv_taps.shape[0]
    half = taps // 2
    padded = with_halo(glu, (("sp", 0),), half)
    filtered = jnp.zeros(glu.shape, jnp.float32) + conv_bias
    for offset in range(taps):
        filtered = (
            filtered + padded[offset : offset + length].astype(jnp.float32) * conv_taps[offset]
        )
    sums, squares = lax.psum(
        (jnp.sum(filtered, axis=-1), jnp.sum(filtered * filtered, axis=-1)), "tp"
    )
    count = chans * lax.axis_size("tp")
    center = (sums / count)[:, None]
    spread = (squares / count)[:, None] - center * center
    conv_out = jax.nn.silu(
        (filtered - center) * lax.rsqrt(spread + 1e-05) * norm_gain + norm_bias
    ).astype(jnp.bfloat16)
    heads_here = head_sink_logit.shape[0]
    head_size = qwidth // heads_here
    kv_here = kwidth // head_size
    query_groups = heads_here // kv_here
    stacked = jnp.stack([key, value_matrix], axis=0)
    banded = with_halo(stacked, (("sp", 1),), WINDOW_REACH)
    span = length + 2 * WINDOW_REACH
    key_band = banded[0].reshape(span, kv_here, head_size)
    value_band = banded[1].reshape(span, kv_here, head_size)
    query4_grouped = query_matrix.reshape(length, kv_here, query_groups, head_size)
    scores = jnp.einsum(
        "qkgd,jkd->kgqj", query4_grouped, key_band, preferred_element_type=jnp.float32
    ) * head_size ** (-0.5)
    offset_pos = lax.axis_index("sp") * length
    seq_len = length * lax.axis_size("sp")
    qpos = offset_pos + jnp.arange(length, dtype=jnp.int32)
    kpos = offset_pos - WINDOW_REACH + jnp.arange(span, dtype=jnp.int32)
    valid = (
        (jnp.abs(qpos[:, None] - kpos[None, :]) <= WINDOW_REACH)
        & (kpos[None, :] >= 0)
        & (kpos[None, :] < seq_len)
    )
    sink_column = head_sink_logit.reshape(kv_here, query_groups, 1)
    masked = jnp.where(valid, scores, -1e30)
    top = jnp.maximum(jnp.max(masked, axis=-1), sink_column)
    expd = jnp.where(valid, jnp.exp(masked - top[..., None]), 0.0)
    total = jnp.sum(expd, axis=-1) + jnp.exp(sink_column - top)
    probs = (expd / total[..., None]).astype(jnp.bfloat16)
    attended = jnp.einsum(
        "kgqj,jkd->qkgd", probs, value_band, preferred_element_type=jnp.float32
    ).astype(jnp.bfloat16)
    attended = attended.reshape(length, qwidth)
    log_total = (top + jnp.log(total)).reshape(heads_here, length).T
    out_conv_cols, out_attn_cols = (
        lax.all_gather(w_out_conv, "sp", axis=1, tiled=True),
        lax.all_gather(w_out_attn, "sp", axis=1, tiled=True),
    )
    out_rows = jnp.concatenate([out_conv_cols, out_attn_cols], axis=0)
    features = jnp.concatenate([conv_out, attended], axis=1)
    mixed = lax.psum_scatter(
        jnp.dot(features, out_rows, preferred_element_type=jnp.float32).astype(jnp.bfloat16),
        "tp",
        scatter_dimension=0,
        tiled=True,
    )
    return (mixed, log_total)


BF = jnp.bfloat16
F32 = jnp.float32


def fused_kernel(
    n, x_hbm, gain_in, wval, wgate, wquery, wkey, wvalue, taps_in, cbias_in, ngain_in, nbias_in,
    sink_in, woc, woa,
    mixed, logt,
    tok, gain, nrm, wc, wq, wo, stc, stq, sto, taps, cbias, ngain, nbias, sink,
    accq, qb, band, keven, kodd, veven, vodd, glu, filt, stat, feat, fe, lgb, lgr, ys, yr, mix,
    lsem, psem, prec, wsem, wrec, vsem, vrec, zsem, zrec, dsem, drec, xsem, xrec, esem, erec, tsem, trec, fsem,
    hsem, hrec, ssem, srec, csem, crec, ysem, yrec, gsem, grec, osem,
):
    sp = lax.axis_index("sp")
    t = lax.axis_index("tp")
    nz = n // 2
    z, x = sp // 2, sp % 2
    y, c = t // 2, t % 2
    sl, tq, slp = 2 * z + c, 2 * y + x, 2 * z + 1 - c
    same, cross = x == c, x != c
    d = (x - c) * (x - c)
    tl, width = x_hbm.shape
    length = 4 * tl
    kb, chans = wval.shape
    qwidth = wquery.shape[1]
    hd = wkey.shape[0]
    kvw = 2 * hd
    heads = sink_in.shape[1]
    ob = woc.shape[1]
    reach = WINDOW_REACH

    def dev(zz, xx, yy, cc):
        return {"sp": 2 * zz + xx, "tp": 2 * yy + cc}

    def rows(o, size):
        return pl.ds(pl.multiple_of(o * size, size), size)

    partner = dev(z, x, y, 1 - c)
    mirror = dev(z, 1 - x, y, 1 - c)
    up, down = dev(z + 1, x, y, c), dev(z - 1, x, y, c)
    has_up, has_down = z < nz - 1, z > 0

    barrier = pltpu.get_barrier_semaphore()

    def hello(to):
        pl.semaphore_signal(barrier, inc=1, device_id=to, device_id_type=pl.DeviceIdType.MESH)

    for e in range(1, 8):
        hello(dev(z, (x + e) % 2, (y + e // 2) % 2, (c + e // 4) % 2))

    @pl.when(has_up)
    def _():
        hello(up)
        hello(dev(z + 1, x, y, 1 - c))

    @pl.when(has_down)
    def _():
        hello(down)
        hello(dev(z - 1, x, y, 1 - c))

    greeted = 7 + 2 * jnp.minimum(nz - 1 - z, 1) + 2 * jnp.minimum(z, 1)

    def when(cond, fn):
        if cond is None:
            fn()
        else:
            pl.when(cond)(fn)

    def local(cond, src, dst, k):
        def make():
            return pltpu.make_async_copy(src, dst, lsem.at[k])

        when(cond, lambda: make().start())
        return lambda: make().wait()

    load_tok = local(None, x_hbm, tok, 0)
    load_gain = local(None, gain_in, gain, 1)
    params = (
        (taps_in, taps), (cbias_in, cbias), (ngain_in, ngain), (nbias_in, nbias), (sink_in, sink)
    )
    load_params = [local(same, src, dst, 2 + i) for i, (src, dst) in enumerate(params)]
    cols = rows(sp, kb)
    per_kind = (
        (
            (wval, wc.at[cols, pl.ds(0, chans)], stc.at[:, pl.ds(0, chans)]),
            (wgate, wc.at[cols, pl.ds(chans, chans)], stc.at[:, pl.ds(chans, chans)]),
        ),
        (
            (wquery, wq.at[sp, pl.ds(0, kb)], stq.at[pl.ds(0, kb)]),
            (wkey, wq.at[sp, pl.ds(kb, hd)], stq.at[pl.ds(kb, hd)]),
            (wvalue, wq.at[sp, pl.ds(kb + hd, hd)], stq.at[pl.ds(kb + hd, hd)]),
        ),
        (
            (woc, wo.at[sp, y, pl.ds(0, chans)], sto.at[pl.ds(0, chans)]),
            (woa, wo.at[sp, y, pl.ds(chans, qwidth)], sto.at[pl.ds(chans, qwidth)]),
        ),
    )
    loaded = []
    k = 7
    for group in per_kind:
        waits = []
        for src, here, there in group:
            waits.append((local(same, src, here, k), local(cross, src, there, k)))
            k += 1
        loaded.append(waits)

    def wait_loaded(kind, which):
        for pair in loaded[kind]:
            pair[which]()

    ends = []

    def remote(spec, cond=None, go=None):
        def make():
            src, dst, ss, rs, to = spec()
            return pltpu.make_async_remote_copy(
                src_ref=src, dst_ref=dst, send_sem=ss, recv_sem=rs, device_id=to,
                device_id_type=pl.DeviceIdType.MESH,
            )

        when(go() if go else None, lambda: make().start())
        ends.append((cond or go, make))

    def arrived(ref, rs, ss):
        pltpu.make_async_remote_copy(
            src_ref=ref, dst_ref=ref, send_sem=ss, recv_sem=rs, device_id=partner,
            device_id_type=pl.DeviceIdType.MESH,
        ).wait_recv()

    qdepth = (kb + kvw) // 2
    cdepth = kb // 2

    def block(k, o, h):
        if k == 0:
            return wc.at[pl.ds(pl.multiple_of(o * kb + h * cdepth, cdepth), cdepth)]
        if k == 1:
            return wq.at[o, pl.ds(pl.multiple_of(h * qdepth, 64), qdepth)]
        return wo.at[o, y, rows(h, chans)]

    def carried(k, zs, e, core):
        return block(k, 2 * zs + (x if e == 0 else 1 - x), core)

    def staged(k, h):
        if k == 0:
            return stc.at[pl.ds(h * cdepth, cdepth)]
        if k == 1:
            return stq.at[pl.ds(h * qdepth, qdepth)]
        return sto.at[pl.ds(h * chans, chans)]

    def hop(k, e, zs, way, cond, go):
        def spec():
            ref = carried(k, zs, e, c)
            to = up if way == 0 else down
            return ref, ref, zsem.at[k, e, zs, way], zrec.at[k, e, zs], to

        remote(spec, cond, go)

    def share(k, e, zs, cond):
        def spec():
            ref = carried(k, zs, e, c)
            return ref, ref, dsem.at[k, e, zs], drec.at[k, e, zs], partner

        remote(spec, cond)

    def across_y(e, zs, cond):
        def spec():
            ref = carried(2, zs, e, c)
            return ref, ref, xsem.at[e, zs], xrec.at[e, zs], dev(z, x, 1 - y, c)

        remote(spec, cond)

    def far_half(e, zs, core):
        return wo.at[2 * zs + (x if e == 0 else 1 - x), 1 - y, rows(core, chans)]

    def from_y(e, zs):
        ref = far_half(e, zs, c)
        arrived(ref, xrec.at[e, zs], xsem.at[e, zs])
        remote(lambda: (ref, ref, esem.at[e, zs], erec.at[e, zs], partner))

    def from_y_shared(e, zs):
        arrived(far_half(e, zs, 1 - c), erec.at[e, zs], esem.at[e, zs])

    mid = has_up & has_down
    low, high = z < nz // 2, z >= nz // 2
    hi = z // 2
    zorder = (z, 4 * hi + 1 - z, 2 - hi, 3 - 3 * hi)

    def flow(k, s, es=(0, 1), only=None, pass_on=True, inner=False):
        below, above = z - s, z + s

        def valid(zs, side):
            ok = (zs >= 0) & (zs <= nz - 1) & side
            return ok & only() if only else ok

        def land(e, zs, way, cond, more, closer):
            arrived(carried(k, zs, e, c), zrec.at[k, e, zs], zsem.at[k, e, zs, way])
            if s < nz - 1 and pass_on:
                hop(k, e, zs, way, lambda: cond() & more, lambda: more)
            if k == 2 and inner:

                @pl.when(closer)
                def _():
                    across_y(e, zs, lambda: cond() & closer)
            elif k == 2:
                across_y(e, zs, cond)
            share(k, e, zs, cond)

        for zs, way, more, closer, side in (
            (above, 1, has_down, low, low),
            (below, 0, has_up, high, low | high),
            (above, 1, has_down, low, high),
        ):
            for e in es:

                @pl.when(valid(zs, side))
                def _():
                    land(
                        e, zs, way, lambda zs=zs, side=side: valid(zs, side), more, closer
                    )

    def shared(k, e, zs):
        arrived(carried(k, zs, e, 1 - c), drec.at[k, e, zs], dsem.at[k, e, zs])

    def all_shared(k, p):
        if p == 0:

            @pl.when(cross)
            def _():
                shared(k, 0, z)
        else:
            shared(k, 0, zorder[p])
        shared(k, 1, zorder[p])

    def swap(k):
        @pl.when(cross)
        def _():
            wait_loaded(k, 1)
            for h in (0, 1):
                remote(
                    lambda h=h: (
                        staged(k, h), block(k, sp, h), wsem.at[k, h], wrec.at[k],
                        dev(z, 1 - x, y, h),
                    ),
                    lambda: cross,
                )

    def give(k):
        @pl.when(same)
        def _():
            wait_loaded(k, 0)
            remote(
                lambda: (
                    block(k, sp, 1 - c), block(k, sp, 1 - c), vsem.at[k], vrec.at[k], partner
                ),
                lambda: same,
            )
            if k < 2:
                hop(k, 0, z, 0, lambda: same & has_up, lambda: has_up)
                hop(k, 0, z, 1, lambda: same & has_down, lambda: has_down)
            share(k, 0, z, lambda: same)

    def given(k):
        @pl.when(cross)
        def _():
            arrived(carried(k, z, 0, c), vrec.at[k], vsem.at[k])
            if k < 2:
                hop(k, 0, z, 0, lambda: cross & has_up, lambda: has_up)
                hop(k, 0, z, 1, lambda: cross & has_down, lambda: has_down)

    def swapped(k):
        arrived(carried(k, z, 1, c), wrec.at[k], wsem.at[k, 0])
        if k < 2:
            hop(k, 1, z, 0, None, lambda: has_up)
            hop(k, 1, z, 1, None, lambda: has_down)
        share(k, 1, z, None)

    jown = 2 * y + c
    across = dev(z, 1 - x, y, x)
    jslot = (1 - d) * jown + 4 * d
    hl = tl // 2

    def half_block(j, h):
        return nrm.at[pl.ds(pl.multiple_of(j * tl + h * hl, hl), hl)]

    def tok_send(e, to, h, cond=None, go=None):
        remote(
            lambda: (
                half_block(jslot, h), half_block(jown, h), tsem.at[e, h], trec.at[jown, h], to
            ),
            cond, go,
        )

    def tok_wait(j, h):
        arrived(half_block(j, h), trec.at[j, h], fsem.at[h])

    load_tok()
    load_gain()
    step = 32

    def norm_body(i, carry):
        r = pl.ds(pl.multiple_of(i * step, step), step)
        flt = tok[r, :].astype(F32)
        scale = lax.rsqrt(jnp.mean(flt * flt, axis=-1, keepdims=True) + 1e-06)
        w = pl.ds(pl.multiple_of(jslot * tl + i * step, step), step)
        nrm[w, :] = (flt * scale * gain[...]).astype(BF)
        return carry

    lax.fori_loop(0, tl // step, norm_body, 0)
    pl.semaphore_wait(barrier, greeted)

    swap(0)
    give(0)
    give(1)
    for h in (0, 1):
        tok_send(0, dev(z, x, 1 - y, x), h)
    for h in (0, 1):
        tok_send(2, partner, h, None, lambda: cross)
    @pl.when(same)
    def _():
        for i, (src, dst) in enumerate(params):
            load_params[i]()
            remote(
                lambda i=i, dst=dst: (dst, dst, psem.at[i], prec.at[i], partner), lambda: same
            )

    @pl.when(cross)
    def _():
        for h in (0, 1):
            tok_send(1, across, h, lambda: cross)

    given(0)
    given(1)
    swapped(0)

    @pl.when(same)
    def _():
        for h in (0, 1):
            tok_send(1, across, h, lambda: same)

    flow(0, 1)
    swap(1)
    jfwd = (1 - d) * (2 * (1 - y) + 1) + d * 2 * y
    fwd_dev = {
        "sp": (1 - d) * (2 * z + 1 - x) + d * sp,
        "tp": (1 - d) * (2 * y + c) + d * (2 * (1 - y) + c),
    }

    def tok_forward(h):
        tok_wait(jfwd, h)
        remote(
            lambda: (
                half_block(jfwd, h), half_block(jfwd, h), fsem.at[h], trec.at[jfwd, h], fwd_dev
            )
        )

    tok_forward(0)
    flow(0, 2)

    tok_forward(1)
    swapped(1)
    swap(2)
    give(2)
    flow(0, 3)
    given(2)
    across_y(0, z, None)

    pad = 16

    def project_conv(yy):
        at = pl.ds(pl.multiple_of(yy * 2 * tl, 2 * tl), 2 * tl)
        res = jnp.dot(nrm[at, :], wc[...], preferred_element_type=F32)
        glu[pl.ds(pl.multiple_of(pad + yy * 2 * tl, pad), 2 * tl), :] = (
            (res[:, 0:chans] * jax.nn.sigmoid(res[:, chans : 2 * chans])).astype(BF).astype(F32)
        )

    for h in (0, 1):
        tok_wait((1 - d) * (2 * y + 1 - c) + d * (2 * y + 1), h)
    for p in range(nz):
        all_shared(0, p)
    def at_mid():
        return mid

    def at_end():
        return jnp.logical_not(mid)

    project_conv(y)
    flow(1, 1, only=at_mid)
    for h in (0, 1):
        tok_wait(2 * (1 - y), h)

    @pl.when(cross)
    def _():
        for h in (0, 1):
            tok_wait(2 * (1 - y) + 1, h)
        for i, (src, dst) in enumerate(params):
            arrived(dst, prec.at[i], psem.at[i])

    project_conv(1 - y)
    zn, zp = jnp.minimum(z + c, nz - 1), jnp.maximum(z - 1 + c, 0)
    nxt, prv = dev(zn, x, y, 1 - c), dev(zp, x, y, 1 - c)
    has_nxt, has_prv = sl < n - 1, sl > 0

    def halo(buf, size, base):
        remote(
            lambda: (
                buf.at[pl.ds(length, size)], buf.at[pl.ds(0, size)], hsem.at[base],
                hrec.at[base], nxt,
            ),
            None, lambda: has_nxt,
        )
        remote(
            lambda: (
                buf.at[pl.ds(size, size)], buf.at[pl.ds(length + size, size)], hsem.at[base + 1],
                hrec.at[base + 1], prv,
            ),
            None, lambda: has_prv,
        )

    def halo_wait(buf, size, base):
        @pl.when(has_prv)
        def _():
            arrived(buf.at[pl.ds(0, size)], hrec.at[base], hsem.at[base])

        @pl.when(has_nxt)
        def _():
            arrived(buf.at[pl.ds(length + size, size)], hrec.at[base + 1], hsem.at[base + 1])

        @pl.when(sl == 0)
        def _():
            buf[pl.ds(0, size), :] = jnp.zeros((size, buf.shape[1]), buf.dtype)

        @pl.when(sl == n - 1)
        def _():
            buf[pl.ds(length + size, size), :] = jnp.zeros((size, buf.shape[1]), buf.dtype)

    halo(glu, pad, 0)
    swapped(2)
    across_y(1, z, None)
    for e in (0, 1):
        hop(2, e, z, 0, None, lambda: low)
        hop(2, e, z, 1, None, lambda: high)
    ntaps = taps.shape[0]
    off = pad - ntaps // 2
    cstep = 64

    def conv_rows(r0):
        acc = jnp.zeros((cstep, chans), F32) + cbias[...]
        for j in range(ntaps):
            acc = acc + glu[pl.ds(r0 + off + j, cstep), :] * taps[pl.ds(j, 1), :]
        filt[pl.ds(r0, cstep), :] = acc

    nconv = length // cstep
    for i in range(1, nconv // 2):
        conv_rows(i * cstep)
    flow(1, 2, only=at_mid)
    for i in range(nconv // 2, nconv - 1):
        conv_rows(i * cstep)
    flow(1, 1, only=at_end)
    halo_wait(glu, pad, 0)
    conv_rows(0)
    conv_rows((nconv - 1) * cstep)
    lane = lax.broadcasted_iota(jnp.int32, (128, 128), 1)
    for b in range(length // 128):
        f = filt[pl.ds(b * 128, 128), :]
        s1 = jnp.sum(f, axis=-1, keepdims=True)
        s2 = jnp.sum(f * f, axis=-1, keepdims=True)
        tile = jnp.where(lane == 0, s1, jnp.where(lane == 1, s2, 0.0))
        stat[pl.ds(tq, 1), :, pl.ds(b * 128, 128)] = jnp.transpose(tile)[None, 0:8, :]
    peers = ((x, 1 - y), (1 - x, 1 - y), (1 - x, y))
    for e, (px, py) in enumerate(peers):
        remote(
            lambda e=e, px=px, py=py: (
                stat.at[tq], stat.at[tq], ssem.at[e], srec.at[tq], dev(z, px, py, c)
            )
        )
    def project_heads(p):
        all_shared(1, p)
        kv, qs = 0.0, 0.0
        for e in (0, 1):
            o = 2 * zorder[p] + e
            lhs = nrm[0:length, rows(o, kb)]
            kv = kv + lax.dot_general(
                lhs, wq[o, kb : kb + kvw, :], (((1,), (1,)), ((), ())), preferred_element_type=F32
            )
            qs = qs + jnp.dot(lhs, wq[o, 0:kb, :], preferred_element_type=F32)
        if p > 0:
            kv = kv + accq[:, qwidth : qwidth + kvw]
            qs = qs + accq[:, 0:qwidth]
        if p < nz - 1:
            accq[:, qwidth : qwidth + kvw] = kv
            accq[:, 0:qwidth] = qs
        else:
            band[pl.ds(reach, length), :] = kv.astype(BF)
            qb[...] = (qs * hd ** (-0.5)).astype(BF)

    for h in (0, 1):
        hop(2, h, z, 0, None, lambda: mid & high)
        hop(2, h, z, 1, None, lambda: mid & low)
    flow(1, 2, only=at_end)
    project_heads(0)
    project_heads(1)
    flow(2, 1, only=at_mid, pass_on=False, inner=True)
    for px, py in peers:
        arrived(stat.at[2 * py + px], srec.at[2 * py + px], ssem.at[0])
    count = chans * 4
    for b in range(length // 128):
        at = pl.ds(b * 128, 128)
        tot = (stat[0, :, at] + stat[1, :, at] + stat[2, :, at] + stat[3, :, at]) / count
        tt = jnp.transpose(jnp.concatenate([tot] * 16, axis=0))
        center = tt[:, 0:1]
        spread = tt[:, 1:2] - center * center
        u = (filt[at, :] - center) * lax.rsqrt(spread + 1e-05)
        u = u * ngain[...] + nbias[...]
        feat[at, 0:chans] = (u * jax.nn.sigmoid(u)).astype(BF)

    def place(j, kind):
        js, cs = j // 2, j % 2
        here = (cs == c) & (js == y)
        away = jnp.logical_not(here)
        r, q = rows(j, tl), pl.ds(kind * chans, chans)
        r2 = rows(c, tl)
        q2 = pl.ds(pl.multiple_of(y * (chans + qwidth) + kind * chans, chans), chans)

        @pl.when(here)
        def _():
            fe[r2, q2] = feat[r, q]

        remote(
            lambda: (
                feat.at[r, q], fe.at[r2, q2], csem.at[kind, j], crec.at[y, kind, c],
                dev(z, x, js, cs),
            ),
            None, lambda: away,
        )

    for j in range(4):
        place(j, 0)
    project_heads(2)
    flow(1, 3)
    project_heads(3)
    halo(band, reach, 2)
    for h in (0, 1):
        hop(2, h, z + 1, 1, None, at_mid)
        hop(2, h, z - 1, 0, None, at_mid)
        from_y(h, z)

    def spread_heads(r0, size):
        at = pl.ds(r0, size)
        b = band[at, :].astype(F32)
        swapped = jnp.concatenate([b[:, hd:], b[:, :hd]], axis=1)
        low = lax.broadcasted_iota(jnp.int32, (size, kvw), 1) < hd
        keven[at, :] = jnp.where(low, b, 0.0).astype(BF)
        vodd[at, :] = jnp.where(low, 0.0, b).astype(BF)
        veven[at, :] = jnp.where(low, swapped, 0.0).astype(BF)
        kodd[at, :] = jnp.where(low, 0.0, swapped).astype(BF)

    spread_heads(reach, length)
    nblk = length // reach
    ri = lax.broadcasted_iota(jnp.int32, (reach, reach), 0)
    ci = lax.broadcasted_iota(jnp.int32, (reach, reach), 1)
    log2e = 1.4426950408889634

    def attend(b):
        span = pl.ds(pl.multiple_of(b * reach, reach), 3 * reach)
        at = rows(b, reach)
        first = reach * (1 - jnp.minimum(sl, 1)) * (1 - jnp.minimum(b, 1))
        last = reach * (1 - jnp.minimum(n - 1 - sl, 1)) * (1 - jnp.minimum(nblk - 1 - b, 1))
        keep_l = ci >= ri + first
        keep_r = ci + last <= ri
        logs = []
        for pair in range(heads // 2):
            q2 = qb[at, pair * kvw : (pair + 1) * kvw]
            acc, inv = None, []
            for e, (kk, vv) in enumerate(((keven, veven), (kodd, vodd))):
                s = lax.dot_general(
                    q2, kk[span, :], (((1,), (1,)), ((), ())), preferred_element_type=F32
                )
                sa = jnp.where(keep_l, s[:, 0:reach], -1e30)
                sb = s[:, reach : 2 * reach]
                sc = jnp.where(keep_r, s[:, 2 * reach :], -1e30)
                h = 2 * pair + e
                sk = sink[0:1, h : h + 1]
                top = jnp.maximum(
                    jnp.max(jnp.maximum(jnp.maximum(sa, sb), sc), axis=-1, keepdims=True), sk
                )
                ea = jnp.exp2((sa - top) * log2e)
                eb = jnp.exp2((sb - top) * log2e)
                ec = jnp.exp2((sc - top) * log2e)
                total = jnp.sum(ea + eb + ec, axis=-1, keepdims=True) + jnp.exp(sk - top)
                p = jnp.concatenate([ea.astype(BF), eb.astype(BF), ec.astype(BF)], axis=1)
                a = jnp.dot(p, vv[span, :], preferred_element_type=F32)
                acc = a if acc is None else acc + a
                inv.append(1.0 / total)
                logs.append(top + jnp.log(total))
            acc = acc * jnp.where(lane < hd, inv[0], inv[1])
            feat[at, chans + pair * kvw : chans + (pair + 1) * kvw] = acc.astype(BF)
        wide = jnp.zeros((reach, 128), F32)
        for h in range(heads):
            wide = jnp.where(lane == h, logs[h], wide)
        lgb[:, at] = jnp.transpose(wide)[0:heads, :]

    far, near = 1 - x, x
    for b in range(1, nblk - 1):
        attend(b)
        place(b, 1)
    halo_wait(band, reach, 2)
    spread_heads(0, reach)
    spread_heads(length + reach, reach)
    flow(2, 1, (0,), at_end)
    attend(0)
    place(0, 1)
    flow(2, 1, (1,), at_end)
    attend(nblk - 1)
    place(nblk - 1, 1)
    outer_z = z - 1 + 2 * hi
    for e in (0, 1):

        def late(e=e):
            ref = carried(2, outer_z, e, c)
            return ref, ref, xsem.at[e, outer_z], xrec.at[e, outer_z], dev(z, x, 1 - y, c)

        remote(late, None, at_mid)

    @pl.when(cross)
    def _():
        remote(lambda: (lgb, lgr, gsem.at[0], grec.at[0], mirror), lambda: cross)

    def gathered(xs):
        for kind in (0, 1):
            for yy, cond in ((y, xs != c), (1 - y, None)):

                def wait(yy=yy, kind=kind):
                    q2 = pl.ds(
                        pl.multiple_of(yy * (chans + qwidth) + kind * chans, chans), chans
                    )
                    arrived(fe.at[rows(xs, tl), q2], crec.at[yy, kind, xs], csem.at[kind, 0])

                when(cond, wait)

    depth = chans + qwidth

    def half_product(js, o):
        lhs = fe[rows(js, tl), :]
        return jnp.dot(lhs[:, 0:depth], wo[o, 0], preferred_element_type=F32) + jnp.dot(
            lhs[:, depth:], wo[o, 1], preferred_element_type=F32
        )

    def column(p, par):
        return 2 * zorder[p] + par

    def emit(p, e):
        par = x if e == 0 else 1 - x
        i = 2 * p + par
        ys[i] = half_product(far, column(p, par)).astype(BF)
        remote(
            lambda: (ys.at[i], yr.at[i], ysem.at[i], yrec.at[i], dev(z, 1 - x, y, c))
        )

    def written(p, par):
        at = rows(column(p, par), ob)
        return pltpu.make_async_copy(mix.at[:, at], mixed.at[:, at], osem.at[2 * p + par])

    def finish(p, e):
        par = 1 - x if e == 0 else x
        i = 2 * p + par
        part = half_product(near, column(p, par))
        arrived(yr.at[i], yrec.at[i], ysem.at[i])
        mix[:, rows(column(p, par), ob)] = (part + yr[i].astype(F32)).astype(BF)
        written(p, par).start()

    flow(2, 2, only=at_mid)
    gathered(far)
    all_shared(2, 0)
    for e in (0, 1):
        from_y_shared(e, z)
        emit(0, e)
    gathered(near)
    steps = [(p, e) for p in range(1, nz) for e in (0, 1)]
    emitted = [(0, 0), (0, 1)]
    done = 0

    def settle(p, e):
        shared(2, e, zorder[p])
        from_y_shared(e, zorder[p])
        emit(p, e)
        emitted.append((p, e))

    for k, (p, e) in enumerate(steps):
        if p < nz - 1:
            flow(2, p + 1, (e,), at_end)
        from_y(e, zorder[p])
        if k > 0:
            settle(*steps[k - 1])
        if len(emitted) - done > 3:
            finish(*emitted[done])
            done += 1
    settle(*steps[-1])
    for u in emitted[done:]:
        finish(*u)

    @pl.when(same)
    def _():
        logt[...] = lgb[...]

    @pl.when(cross)
    def _():
        arrived(lgr, grec.at[0], gsem.at[0])
        logt[...] = lgr[...]

    for p in range(nz):
        for par in (0, 1):
            written(p, par).wait()
    for cond, make in ends:
        when(cond() if cond else None, lambda make=make: make().wait_send())


def layer(
    n, parts, tokens, in_gain, w_conv_val, w_conv_gate, w_query, w_key, value_weight, conv_taps,
    conv_bias, norm_gain, norm_bias, head_sink_logit, w_out_conv, w_out_attn,
):
    tl, width = tokens.shape
    kb, chans = w_conv_val.shape
    qwidth = w_query.shape[1]
    kvw = 2 * w_key.shape[1]
    heads = head_sink_logit.shape[0]
    ob = w_out_conv.shape[1]
    fits = (
        parts == 4 and n == 8 and tl % 128 == 0 and kb % 128 == 0 and ob % 128 == 0 and n * ob == width and chans == qwidth
        and chans % 128 == 0 and kvw == 128 and kb == qwidth and qwidth == heads * kvw // 2
        and conv_taps.shape[0] <= 33 and heads % 2 == 0
    )
    if not fits:
        return on_device(
            tokens, in_gain, w_conv_val, w_conv_gate, w_query, w_key, value_weight, conv_taps,
            conv_bias, norm_gain, norm_bias, head_sink_logit, w_out_conv, w_out_attn,
        )
    length = 4 * tl
    nz = n // 2
    vm = pl.BlockSpec(memory_space=pltpu.VMEM)
    hb = pl.BlockSpec(memory_space=pl.ANY)
    dma = pltpu.SemaphoreType.DMA
    mixed, log_rows = pl.pallas_call(
        functools.partial(fused_kernel, n),
        out_shape=(
            jax.ShapeDtypeStruct((tl, width), BF),
            jax.ShapeDtypeStruct((heads, length), F32),
        ),
        in_specs=[hb] * 14,
        out_specs=(hb, vm),
        scratch_shapes=[
            pltpu.VMEM((tl, width), BF),
            pltpu.VMEM((1, width), F32),
            pltpu.VMEM((5 * tl, width), BF),
            pltpu.VMEM((n * kb, 2 * chans), BF),
            pltpu.VMEM((n, kb + kvw, qwidth), BF),
            pltpu.VMEM((n, 2, chans + qwidth, ob), BF),
            pltpu.VMEM((kb, 2 * chans), BF),
            pltpu.VMEM((kb + kvw, qwidth), BF),
            pltpu.VMEM((chans + qwidth, ob), BF),
            pltpu.VMEM(conv_taps.shape, F32),
            pltpu.VMEM((1, chans), F32),
            pltpu.VMEM((1, chans), F32),
            pltpu.VMEM((1, chans), F32),
            pltpu.VMEM((1, heads), F32),
            pltpu.VMEM((length, qwidth + kvw), F32),
            pltpu.VMEM((length, qwidth), BF),
            *[pltpu.VMEM((length + 2 * WINDOW_REACH, kvw), BF)] * 5,
            pltpu.VMEM((length + 32, chans), F32),
            pltpu.VMEM((length, chans), F32),
            pltpu.VMEM((4, 8, length), F32),
            pltpu.VMEM((length, chans + qwidth), BF),
            pltpu.VMEM((2 * tl, 2 * (chans + qwidth)), BF),
            pltpu.VMEM((heads, length), F32),
            pltpu.VMEM((heads, length), F32),
            pltpu.VMEM((n, tl, ob), BF),
            pltpu.VMEM((n, tl, ob), BF),
            pltpu.VMEM((tl, width), BF),
            dma((14,)),
            dma((5,)),
            dma((5,)),
            dma((3, 2)),
            dma((3,)),
            dma((3,)),
            dma((3,)),
            dma((3, 2, nz, 2)),
            dma((3, 2, nz)),
            dma((3, 2, nz)),
            dma((3, 2, nz)),
            dma((2, nz)),
            dma((2, nz)),
            dma((2, nz)),
            dma((2, nz)),
            dma((3, 2)),
            dma((4, 2)),
            dma((3,)),
            dma((4,)),
            dma((4,)),
            dma((3,)),
            dma((4,)),
            dma((2, 4)),
            dma((2, 2, 2)),
            dma((n,)),
            dma((n,)),
            dma((1,)),
            dma((1,)),
            dma((n,)),
        ],
        compiler_params=pltpu.CompilerParams(
            collective_id=0, has_side_effects=True, vmem_limit_bytes=56 * 1024 * 1024
        ),
    )(
        tokens, in_gain.reshape(1, width), w_conv_val, w_conv_gate, w_query, w_key.T, value_weight.T,
        conv_taps, conv_bias.reshape(1, chans), norm_gain.reshape(1, chans), norm_bias.reshape(1, chans),
        head_sink_logit.reshape(1, heads), w_out_conv, w_out_attn,
    )
    return mixed, log_rows.T


def solution(mesh):
    return jax.shard_map(
        functools.partial(layer, mesh.shape["sp"], mesh.shape["tp"]),
        mesh=mesh,
        in_specs=(
            P(("sp", "tp"), None),
            P(),
            P("sp", "tp"),
            P("sp", "tp"),
            P("sp", "tp"),
            P("sp", "tp"),
            P("sp", "tp"),
            P(None, "tp"),
            P("tp"),
            P("tp"),
            P("tp"),
            P("tp"),
            P("tp", "sp"),
            P("tp", "sp"),
        ),
        out_specs=(P(("sp", "tp"), None), P("sp", "tp")),
        check_vma=False,
    )
```

time: 77.6 us -> 76 us (0.979)
  Pallas kernels: 74.3 us -> 72.7 us
    pallas_call x1, Pallas kernels: 74.3 us -> 72.7 us  [layer(): pl.pallas_call(functools.partial(fused_kernel, n), out_shape=(jax.ShapeDt...]
where the time goes in v1:
time: 76 us; the launch traced here: 75.8 us
  Pallas kernels  72.7 us (96%)
  local copies, waits for them, and re-layouts  2.49 us (3%)
    pallas_call x1, Pallas kernels, layer(): pl.pallas_call(functools.partial(fused_kernel, n), out_shape=(jax.ShapeDt...  72.7 us
    unnamed x4, local copies, waits for them, and re-layouts  2.49 us

profile of v1, /device:TPU:0, one launch (start us, length us, event | category | flops | bytes accessed | tf_op | source)
XLA Modules:
  0.0 75.8 jit_solution(18000471652483107080)
XLA Ops:
  0.6 72.7 %shard_map.149 = (bf16[128,2048]{1,0:T(8,128)(2,1)}, f32[4,512]{1,0:T(4,128)}) custom-call(bf16[128,2048]{1,0:T(8,128)(2,1)} %x_hbm.1, f32[1,2048]{1,0:T(1,128)} %bitcast.10, bf16[256,256]{1,0:T(8,128)(2,1)} %wval.1, bf16[256,256]{1,0:T(8,128)(2,1)} %wgate.1, bf16[256,256]{1,0:T(8,128)(2,1)} %wquery.1, bf16[64,256]{1,0:T(8,128)(2,1)} %bitcast.8, ...), custom_call_target="tpu_custom_call" | custom-call | tf_op jit(solution)/shard_map/pallas_call | solution.py:878
  73.3 0.0 copy-start
  73.3 1.9 %copy.18 = bf16[128,2048]{1,0:T(8,128)(2,1)} copy(bf16[128,2048]{1,0:T(8,128)(2,1)} %get-tuple-element.8) | data formatting | bytes 1048576
  75.2 0.0 copy-done
  75.2 0.6 copy.19
Async XLA Ops:
  73.3 1.9 %copy-start = (f32[4,512]{1,0:T(4,128)S(1)}, f32[4,512]{1,0:T(4,128)}, u32[]{:S(2)}) copy-start(f32[4,512]{1,0:T(4,128)} %get-tuple-element.5) | copy-start | bytes 24580
